TPU v7x, 32 devices: a whole 2x2x4 slice. The times are simulated.
32 devices in a mesh: fs: 16 (over z, y, x), tp: 2 (over core).
Axes of the slice: x: 2, y: 2, z: 4, core: 2. Of those that a mesh axis runs over, the one named last changes fastest.
Arguments:
- tokens: bfloat16 [4096, 2048], P('fs'), may hold values from -6 to 6
- mix_gain: float32 [2048], replicated, may hold values from 0.1 to 1.9
- glu_value: bfloat16 [2048, 2048], P('fs', 'tp'), may hold values from -0.125 to 0.125
- glu_gate: bfloat16 [2048, 2048], P('fs', 'tp'), may hold values from -0.125 to 0.125
- conv_taps: float32 [31, 2048], P(None, 'tp'), may hold values from -2.2 to 2.2, as said below
- chan_gain: float32 [2048], P('tp'), may hold values from 0.1 to 1.9
- mix_out: bfloat16 [2048, 2048], P('tp', 'fs'), may hold values from -0.125 to 0.125
- mlp_gain: float32 [2048], replicated, may hold values from 0.1 to 1.9
- up_weight: bfloat16 [2048, 8192], P('fs', 'tp'), may hold values from -0.125 to 0.125
- down_weight: bfloat16 [8192, 2048], P('tp', 'fs'), may hold values from -0.0625 to 0.0625
Outputs:
- result: bfloat16 [4096, 2048], P('fs')
Inputs may be any that keep to these rules, and one draw needn't show every extreme that they name: `conv_taps`: independent entries scaled by fan-in; channels fall into 16 groups of different scale.
All inputs are finite; a program needn't handle non-finite values.
Results may differ from a plain program's by a relative error of at most 0.018.
Values may be sent and summed in bfloat16 or wider, within the bound.
No kernel may reach another device: no remote copies, remote signals or barrier semaphores. Data moves between devices by JAX's collectives and lax.ppermute only.
A program may use at most 128 MiB of HBM per device.

v0:
```python
import jax
import jax.numpy as jnp
from jax import lax
from jax.sharding import PartitionSpec as P

C = 2048
LEN = 128


norm_floor = 0.05


def rms_scale(stream, gain):
    return stream * lax.rsqrt(jnp.mean(stream * stream, axis=-1, keepdims=True) + norm_floor) * gain


def bf16_round(value):
    return lax.optimization_barrier(value.astype(jnp.bfloat16)).astype(jnp.float32)


def depthwise(glu, conv_taps):
    seqs = glu.shape[0] // LEN
    blocks = glu.reshape(seqs, LEN, glu.shape[1]).astype(jnp.float32)
    reach = conv_taps.shape[0] // 2
    padded = jnp.pad(blocks, ((0, 0), (reach, reach), (0, 0)))
    total = jnp.zeros_like(blocks)
    for offset in range(conv_taps.shape[0]):
        total = total + padded[:, offset : offset + LEN] * conv_taps[offset]
    return total.reshape(glu.shape)


def per_device(
    tokens,
    mix_gain,
    glu_value,
    glu_gate,
    conv_taps,
    chan_gain,
    mix_out,
    mlp_gain,
    up_weight,
    down_weight,
):
    stream = tokens.astype(jnp.float32)
    normed = rms_scale(stream, mix_gain).astype(jnp.bfloat16)
    values = jnp.dot(
        normed,
        lax.all_gather(glu_value, "fs", axis=0, tiled=True),
        preferred_element_type=jnp.float32,
    )
    gating = jnp.dot(
        normed,
        lax.all_gather(glu_gate, "fs", axis=0, tiled=True),
        preferred_element_type=jnp.float32,
    )
    glu = (values * jax.nn.sigmoid(gating)).astype(jnp.bfloat16)
    convolved = depthwise(glu, conv_taps)
    sums, squares = lax.psum(
        (jnp.sum(convolved, axis=-1), jnp.sum(convolved * convolved, axis=-1)), "tp"
    )
    centre = (sums / C)[:, None]
    spread = (squares / C)[:, None] - centre * centre
    hidden = jax.nn.silu((convolved - centre) * lax.rsqrt(spread + norm_floor) * chan_gain).astype(
        jnp.bfloat16
    )
    whole_out = lax.all_gather(mix_out, "fs", axis=1, tiled=True)
    own_rows = stream.shape[0] // lax.axis_size("tp")
    mixed = lax.psum_scatter(
        jnp.dot(hidden, whole_out, preferred_element_type=jnp.float32).astype(jnp.bfloat16),
        "tp",
        scatter_dimension=0,
        tiled=True,
    ).astype(jnp.float32)
    own_stream = lax.dynamic_slice_in_dim(stream, lax.axis_index("tp") * own_rows, own_rows, 0)
    resid = own_stream + bf16_round(mixed)
    normed_mlp = rms_scale(resid, mlp_gain).astype(jnp.bfloat16)
    whole_up = lax.all_gather(up_weight, "fs", axis=0, tiled=True)
    active = jnp.square(
        jax.nn.relu(
            jnp.dot(
                lax.all_gather(normed_mlp, "tp", axis=0, tiled=True),
                whole_up,
                preferred_element_type=jnp.float32,
            )
        )
    ).astype(jnp.bfloat16)
    whole_down = lax.all_gather(down_weight, "fs", axis=1, tiled=True)
    feed = lax.psum_scatter(
        jnp.dot(active, whole_down, preferred_element_type=jnp.float32).astype(jnp.bfloat16),
        "tp",
        scatter_dimension=0,
        tiled=True,
    ).astype(jnp.float32)
    finished = (resid + bf16_round(feed)).astype(jnp.bfloat16)
    return lax.all_gather(finished, "tp", axis=0, tiled=True)


def solution(mesh):
    in_specs = (
        P("fs", None),
        P(),
        P("fs", "tp"),
        P("fs", "tp"),
        P(None, "tp"),
        P("tp"),
        P("tp", "fs"),
        P(),
        P("fs", "tp"),
        P("tp", "fs"),
    )
    out_specs = P("fs", None)
    return jax.shard_map(
        per_device, mesh=mesh, in_specs=in_specs, out_specs=out_specs, check_vma=False
    )
```

profile of v0, /device:TPU:0, one launch (start us, length us, event | category | flops | bytes accessed | tf_op | source)
XLA Modules:
  0.0 769.7 jit_solution(15755725362399529471)
XLA Ops:
  6.5 0.7 all-gather.10.cloned.1.call-update
  7.3 0.7 all-gather.8.cloned.1.call-update
  8.1 0.7 all-gather.12.cloned.1.call-update
  8.8 1.5 multiply_reduce_fusion
  10.3 1.1 fusion.72
  11.4 1.4 fusion.71
  12.9 75.6 %all-gather.10.cloned.1.call-done = bf16[2048,1024]{1,0:T(8,128)(2,1)} async-done(((bf16[128,1024]{1,0:T(8,128)(2,1)}), bf16[2048,1024]{1,0:T(8,128)(2,1)}) %all-gather.10.cloned.1.call-update) | async-done | bytes 4194320 | tf_op jit(solution)/shard_map/all_gather | solution.py:53
  88.4 3.9 fusion.4
  92.4 73.1 %all-gather.8.cloned.1.call-done = bf16[2048,1024]{1,0:T(8,128)(2,1)} async-done(((bf16[128,1024]{1,0:T(8,128)(2,1)}), bf16[2048,1024]{1,0:T(8,128)(2,1)}) %all-gather.8.cloned.1.call-update) | async-done | bytes 4194320 | tf_op jit(solution)/shard_map/all_gather | solution.py:48
  165.4 3.5 bitcast_convert_fusion
  169.0 5.7 fusion.69
  174.7 2.5 all-reduce.1
  177.2 0.4 multiply_convert_fusion.2
  177.6 77.9 %all-gather.12.cloned.1.call-done = bf16[1024,2048]{1,0:T(8,128)(2,1)} async-done(((bf16[1024,128]{1,0:T(8,128)(2,1)}), bf16[1024,2048]{1,0:T(8,128)(2,1)}) %all-gather.12.cloned.1.call-update) | async-done | bytes 4194320 | tf_op jit(solution)/shard_map/all_gather | solution.py:66
  255.5 4.4 convolution_convert_fusion.1
  259.9 0.0 all-gather.14.cloned.1.call-start
  260.0 0.2 convert_element_type.45
  260.2 6.4 reduce-scatter.3.cloned.1.call-done
  266.7 1.3 multiply_reduce_fusion.1
  267.9 2.0 multiply_convert_fusion.1
  270.0 0.0 all-gather.16.cloned.1.call-start
  270.0 0.5 all-gather.16.cloned.1.call-update
  270.6 0.7 all-gather.18.cloned.1.call-update
  271.4 9.0 %all-gather.14.cloned.1.call-done = bf16[256,2048]{1,0:T(8,128)(2,1)} async-done(((bf16[128,2048]{1,0:T(8,128)(2,1)}), bf16[256,2048]{1,0:T(8,128)(2,1)}) %all-gather.14.cloned.1.call-update) | async-done | bytes 1048592 | tf_op jit(solution)/shard_map/all_gather | solution.py:81
  280.4 194.8 %all-gather.16.cloned.1.call-done = bf16[2048,4096]{1,0:T(8,128)(2,1)} async-done(((bf16[128,4096]{1,0:T(8,128)(2,1)}), bf16[2048,4096]{1,0:T(8,128)(2,1)}) %all-gather.16.cloned.1.call-update) | async-done | bytes 16777232 | tf_op jit(solution)/shard_map/all_gather | solution.py:77
  475.2 250.0 %all-gather.18.cloned.1.call-done = bf16[4096,2048]{1,0:T(8,128)(2,1)} async-done(((bf16[4096,128]{1,0:T(8,128)(2,1)}), bf16[4096,2048]{1,0:T(8,128)(2,1)}) %all-gather.18.cloned.1.call-update) | async-done | bytes 16777232 | tf_op jit(solution)/shard_map/all_gather | solution.py:87
  725.2 16.4 %convolution_convert_fusion = bf16[256,2048]{1,0:T(8,128)(2,1)} fusion(bf16[4096,2048]{1,0:T(8,128)(2,1)} %all-gather.18.cloned.1.call-done, bf16[256,2048]{1,0:T(8,128)(2,1)} %all-gather.14.cloned.1.call-done, bf16[2048,4096]{1,0:T(8,128)(2,1)} %all-gather.16.cloned.1.call-done), kind=kOutput, calls=%fused_computation.33 | convolution fusion | flops 8593604608 | bytes 35651584 | tf_op jit(solution)/shard_map/dot_general | solution.py:89
  741.7 0.0 all-gather.20.cloned.1.call-start
  741.8 6.7 reduce-scatter.5.cloned.1.call-done
  748.4 2.0 add_convert_fusion
  750.5 10.4 %all-gather.20.cloned.1.call-done = bf16[256,2048]{1,0:T(8,128)(2,1)} async-done(((bf16[128,2048]{1,0:T(8,128)(2,1)}), bf16[256,2048]{1,0:T(8,128)(2,1)}) %all-gather.20.cloned.1.call-update) | async-done | bytes 1048592 | tf_op jit(solution)/shard_map/all_gather | solution.py:95
  760.9 2.3 copy.12
  (23 shorter events, 0.3 us)
Async XLA Ops:
  6.5 81.9 %all-gather.10.cloned.1.call-start = ((), (), s32[]{:S(2)}) async-start(), calls=%async_computation.3 | async-start | bytes 4456448 | tf_op jit(solution)/shard_map/all_gather | solution.py:53
  7.3 158.2 %all-gather.8.cloned.1.call-start = ((), (), s32[]{:S(2)}) async-start(), calls=%async_computation.2 | async-start | bytes 4456448 | tf_op jit(solution)/shard_map/all_gather | solution.py:48
  8.0 247.5 %all-gather.12.cloned.1.call-start = ((), (), s32[]{:S(2)}) async-start(), calls=%async_computation.4 | async-start | bytes 4456448 | tf_op jit(solution)/shard_map/all_gather | solution.py:66
  8.7 257.9 %reduce-scatter.3.cloned.1.call-start = ((), (), s32[]{:S(2)}) async-start(), calls=%async_computation.5 | async-start | bytes 1572864 | tf_op jit(solution)/shard_map/reduce_scatter | solution.py:68
  12.8 152.6 %copy-start.1 = (bf16[256,2048]{1,0:T(8,128)(2,1)S(1)}, bf16[256,2048]{1,0:T(8,128)(2,1)}, u32[]{:S(2)}) copy-start(bf16[256,2048]{1,0:T(8,128)(2,1)} %param.10) | copy-start | bytes 3145732
  12.8 152.6 %copy-start.4 = (f32[2048]{0:T(1024)S(1)}, f32[2048]{0:T(1024)}, u32[]{:S(2)}) copy-start(f32[2048]{0:T(1024)} %param.11) | copy-start | bytes 24580
  92.4 84.8 %copy-start.3 = (f32[1024]{0:T(1024)S(1)}, f32[1024]{0:T(1024)}, u32[]{:S(2)}) copy-start(f32[1024]{0:T(1024)} %param.15) | copy-start | bytes 12292
  259.9 8.0 %copy-start.2 = (f32[2048]{0:T(1024)S(1)}, f32[2048]{0:T(1024)}, u32[]{:S(2)}) copy-start(f32[2048]{0:T(1024)} %param.17) | copy-start | bytes 24580
  259.9 20.4 %all-gather.14.cloned.1.call-start = ((), (), s32[]{:S(2)}) async-start(), calls=%async_computation.6 | async-start | bytes 1572864 | tf_op jit(solution)/shard_map/all_gather | solution.py:81
  270.0 205.2 %all-gather.16.cloned.1.call-start = ((), (), s32[]{:S(2)}) async-start(), calls=%async_computation.7 | async-start | bytes 17825792 | tf_op jit(solution)/shard_map/all_gather | solution.py:77
  270.6 454.7 %all-gather.18.cloned.1.call-start = ((), (), s32[]{:S(2)}) async-start(), calls=%async_computation.8 | async-start | bytes 17825792 | tf_op jit(solution)/shard_map/all_gather | solution.py:87
  271.3 477.1 %copy-start = (bf16[128,2048]{1,0:T(8,128)(2,1)S(1)}, bf16[128,2048]{1,0:T(8,128)(2,1)}, u32[]{:S(2)}) copy-start(bf16[128,2048]{1,0:T(8,128)(2,1)} %reduce-scatter.3.cloned.1.call-done) | copy-start | bytes 1572868
  271.3 477.1 %reduce-scatter.5.cloned.1.call-start = ((), (), s32[]{:S(2)}) async-start(), calls=%async_computation.9 | async-start | bytes 1572864 | tf_op jit(solution)/shard_map/reduce_scatter | solution.py:88
  741.7 19.2 %all-gather.20.cloned.1.call-start = ((), (), s32[]{:S(2)}) async-start(), calls=%async_computation.10 | async-start | bytes 1572864 | tf_op jit(solution)/shard_map/all_gather | solution.py:95
Sparse Core Ops, SparseCore 0:
  10.1 78.3 all-gather.9
  91.2 74.1 all-gather.7
  168.1 87.3 all-gather.11
  260.1 6.5 reduce-scatter.2
  270.1 10.2 all-gather.13
  283.0 192.1 all-gather.15
  477.9 247.2 all-gather.17
  741.8 6.5 reduce-scatter.4
  750.6 10.2 all-gather.19
where the time goes:
time: 770 us
  waiting for transfers between devices  707 us (92%)
  matrix products  28.3 us (4%)
  between operations  13.3 us (2%)
  other arithmetic  13.2 us (2%)
    all_gather x1, waiting for transfers between devices, per_device(): whole_down = lax.all_gather(down_weight, 'fs', axis=1, tiled=True)  250 us
    all_gather x1, waiting for transfers between devices, per_device(): whole_up = lax.all_gather(up_weight, 'fs', axis=0, tiled=True)  195 us
    all_gather x1, waiting for transfers between devices, per_device(): whole_out = lax.all_gather(mix_out, 'fs', axis=1, tiled=True)  77.9 us
    all_gather x1, waiting for transfers between devices, per_device(): lax.all_gather(glu_gate, 'fs', axis=0, tiled=True)  75.6 us
    all_gather x1, waiting for transfers between devices, per_device(): lax.all_gather(glu_value, 'fs', axis=0, tiled=True)  73.1 us
    dot_general x1, matrix products, per_device(): jnp.dot(active, whole_down, preferred_element_type=jnp.float32)  16.4 us
  transfers between devices with their start and end apart: 9, of which 9 were waited for; matrix products, arithmetic and copies ran while one was open for 2% of the time, Pallas kernels for 0%

commit v1 on v0

v1 whole, which is shorter than its diff:
```python
import math

import jax
import jax.numpy as jnp
from jax import lax
from jax.sharding import PartitionSpec as P

LEN = 128
norm_floor = 0.05


def rms_scale(stream, gain):
    return stream * lax.rsqrt(jnp.mean(stream * stream, axis=-1, keepdims=True) + norm_floor) * gain


def bf16_round(value):
    return lax.optimization_barrier(value.astype(jnp.bfloat16)).astype(jnp.float32)


def depthwise(glu, taps):
    s, tokens, c = glu.shape
    blocks = glu.reshape(s, tokens // LEN, LEN, c).astype(jnp.float32)
    reach = taps.shape[0] // 2
    padded = jnp.pad(blocks, ((0, 0), (0, 0), (reach, reach), (0, 0)))
    total = jnp.zeros_like(blocks)
    for offset in range(taps.shape[0]):
        total = total + padded[:, :, offset : offset + LEN] * taps[offset][:, None, None]
    return total.reshape(glu.shape)


class Plan:
    def __init__(self, mesh, rows):
        self.fs, self.tp = mesh.shape["fs"], mesh.shape["tp"]
        self.plane = math.gcd(self.fs, 4)
        self.lines = self.fs // self.plane
        self.split = math.gcd(self.tp, rows // LEN)
        self.other = self.tp // self.split
        m, k, s, h = self.plane, self.lines, self.split, self.other
        self.plane_groups = [[z * m + q for q in range(m)] for z in range(k)]
        self.line_groups = [
            [(z * m + q) * self.tp + o * s + j for j in range(s) for z in range(k)]
            for q in range(m)
            for o in range(h)
        ]
        self.token_groups = [
            [(z * m + q) * self.tp + o * s + j for q in range(m) for o in range(h)]
            for z in range(k)
            for j in range(s)
        ]
        self.split_groups = [[o * s + j for j in range(s)] for o in range(h)]
        self.other_groups = [[o * s + j for o in range(h)] for j in range(s)]

    def exchange(self, x):
        return lax.all_to_all(
            x, "fs", axis_index_groups=self.plane_groups, split_axis=0, concat_axis=0, tiled=True
        )

    def weight(self, x):
        x = self.exchange(x).reshape(-1, x.shape[-1])
        x = lax.all_gather(
            x, ("fs", "tp"), axis_index_groups=self.line_groups, axis=0, tiled=True
        )
        return x.reshape(self.split, -1, x.shape[-1])

    def share(self, x):
        wide = jnp.broadcast_to(x[None], (self.plane,) + x.shape)
        return self.exchange(wide).reshape(-1, x.shape[-1])

    def reduce(self, x):
        x = self.exchange(x.reshape(self.plane, -1, x.shape[-1])).astype(jnp.float32)
        total = jnp.sum(x, axis=0)
        if self.other > 1:
            total = lax.psum(total, "tp", axis_index_groups=self.other_groups)
        return total


def columns(x, parts):
    return jnp.transpose(x.reshape(x.shape[0], parts, -1), (1, 0, 2))


def rows_t(x, parts):
    return jnp.transpose(x.reshape(parts, -1, x.shape[1]), (0, 2, 1))


def build(plan):
    def per_device(
        tokens,
        mix_gain,
        glu_value,
        glu_gate,
        conv_taps,
        chan_gain,
        mix_out,
        mlp_gain,
        up_weight,
        down_weight,
    ):
        m, s = plan.plane, plan.split
        place = lax.axis_index("tp") % s
        member = lax.axis_index("fs") % m
        own = tokens.shape[0] // s
        stream = lax.dynamic_slice_in_dim(tokens, place * own, own, 0).astype(jnp.float32)
        channels = glu_value.shape[1] * plan.tp

        w_glu = plan.weight(
            jnp.concatenate([columns(glu_value, m), columns(glu_gate, m)], axis=2)
        )
        w_mix = plan.weight(rows_t(mix_out, m))
        w_up = plan.weight(columns(up_weight, m))
        w_down = plan.weight(rows_t(down_weight, m))
        cq = w_mix.shape[2]

        small = jnp.concatenate([conv_taps, chan_gain[None]], axis=0)
        small = lax.dynamic_slice_in_dim(small, member * cq, cq, 1)
        small = lax.all_gather(small, "tp", axis_index_groups=plan.split_groups, axis=1)
        taps, gain = small[:-1], small[-1]

        normed = plan.share(rms_scale(stream, mix_gain).astype(jnp.bfloat16))
        both = jnp.einsum("td,sdn->stn", normed, w_glu, preferred_element_type=jnp.float32)
        glu = (both[..., :cq] * jax.nn.sigmoid(both[..., cq:])).astype(jnp.bfloat16)
        convolved = depthwise(glu, taps)
        sums, squares = lax.psum(
            (jnp.sum(convolved, axis=(0, 2)), jnp.sum(convolved * convolved, axis=(0, 2))),
            ("fs", "tp"),
            axis_index_groups=plan.token_groups,
        )
        centre = (sums / channels)[:, None]
        spread = (squares / channels)[:, None] - centre * centre
        hidden = jax.nn.silu(
            (convolved - centre) * lax.rsqrt(spread + norm_floor) * gain[:, None]
        ).astype(jnp.bfloat16)
        mixed = plan.reduce(
            jnp.einsum("stc,sdc->td", hidden, w_mix, preferred_element_type=jnp.float32).astype(
                jnp.bfloat16
            )
        )
        resid = stream + bf16_round(mixed)
        normed_mlp = plan.share(rms_scale(resid, mlp_gain).astype(jnp.bfloat16))
        active = jnp.square(
            jax.nn.relu(
                jnp.einsum("td,sdf->stf", normed_mlp, w_up, preferred_element_type=jnp.float32)
            )
        ).astype(jnp.bfloat16)
        feed = plan.reduce(
            jnp.einsum("stf,sdf->td", active, w_down, preferred_element_type=jnp.float32).astype(
                jnp.bfloat16
            )
        )
        finished = (resid + bf16_round(feed)).astype(jnp.bfloat16)
        whole = jnp.zeros((s,) + finished.shape, finished.dtype)
        whole = lax.dynamic_update_slice_in_dim(whole, finished[None], place, 0)
        for step in range(1, s):
            pairs = [
                (group[j], group[(j + step) % s]) for group in plan.split_groups for j in range(s)
            ]
            piece = lax.ppermute(finished, "tp", pairs)
            whole = lax.dynamic_update_slice_in_dim(whole, piece[None], (place - step) % s, 0)
        return whole.reshape(tokens.shape)

    return per_device


def solution(mesh):
    in_specs = (
        P("fs", None),
        P(),
        P("fs", "tp"),
        P("fs", "tp"),
        P(None, "tp"),
        P("tp"),
        P("tp", "fs"),
        P(),
        P("fs", "tp"),
        P("tp", "fs"),
    )
    out_specs = P("fs", None)

    def step(tokens, *rest):
        plan = Plan(mesh, tokens.shape[0] // mesh.shape["fs"])
        return jax.shard_map(
            build(plan), mesh=mesh, in_specs=in_specs, out_specs=out_specs, check_vma=False
        )(tokens, *rest)

    return step
```

time: 770 us -> 322 us (0.42)
  waiting for transfers between devices: 707 us -> 148 us
  blocking collectives: 2.47 us -> 107 us
    all_gather x7 -> x4, waiting for transfers between devices: 691 us -> 103 us  [weight(): lax.all_gather(x, ('fs', 'tp'), axis_index_groups=self.line_groups, axis=...]
    all_to_all x0 -> x6, blocking collectives: none -> 96.3 us  [exchange(): lax.all_to_all(x, 'fs', axis_index_groups=self.plane_groups, split_axis=0...]
    all_to_all x0 -> x2, waiting for transfers between devices: none -> 43.1 us  [exchange(): lax.all_to_all(x, 'fs', axis_index_groups=self.plane_groups, split_axis=0...]
    reduce_scatter x2 -> x0, waiting for transfers between devices: 13.1 us -> none  [the longest x1 6.68 us: per_device(): lax.psum_scatter(jnp.dot(active, whole_down, preferred_element_type=jnp.f...]
    dot_general x4 -> x3, matrix products: 28.3 us -> 23.6 us  [the longest x1 15.9 us: per_device(): jnp.einsum('stf,sdf->td', active, w_down, preferred_element_type=jnp.floa...]
  transfers between devices with their start and end apart: 9 -> 7, of which waited for: 9 -> 5; matrix products, arithmetic and copies ran while one was open for 2% -> 7% of each run, Pallas kernels for 0% -> 0%
where the time goes in v1:
time: 322 us; the launch traced here: 321 us
  waiting for transfers between devices  148 us (46%)
  blocking collectives  107 us (33%)
  matrix products  23.6 us (7%)
  between operations  13.4 us (4%)
  other arithmetic  10.5 us (3%)
  local copies, waits for them, and re-layouts  10.3 us (3%)
  starting transfers between devices  7.58 us (2%)
    all_gather x4, waiting for transfers between devices, weight(): lax.all_gather(x, ('fs', 'tp'), axis_index_groups=self.line_groups, axis=...  103 us
    all_to_all x6, blocking collectives, exchange(): lax.all_to_all(x, 'fs', axis_index_groups=self.plane_groups, split_axis=0...  96.3 us
    all_to_all x2, waiting for transfers between devices, exchange(): lax.all_to_all(x, 'fs', axis_index_groups=self.plane_groups, split_axis=0...  43.1 us
    dot_general x1, matrix products, per_device(): jnp.einsum('stf,sdf->td', active, w_down, preferred_element_type=jnp.floa...  15.9 us
    psum x1, blocking collectives, per_device(): lax.psum((jnp.sum(convolved, axis=(0, 2)), jnp.sum(convolved * convolved,...  8.89 us
    all_to_all x2, starting transfers between devices, exchange(): lax.all_to_all(x, 'fs', axis_index_groups=self.plane_groups, split_axis=0...  7.39 us
  transfers between devices with their start and end apart: 7, of which 5 were waited for; matrix products, arithmetic and copies ran while one was open for 7% of the time, Pallas kernels for 0%

profile of v1, /device:TPU:0, one launch (start us, length us, event | category | flops | bytes accessed | tf_op | source)
XLA Modules:
  0.0 320.8 jit_solution(10173680697015407925)
XLA Ops:
  6.5 1.1 copy.26
  7.7 1.2 copy.27
  9.1 13.8 %all_to_all.40 = bf16[4,128,512]{2,1,0:T(8,128)(2,1)} all-to-all(bf16[4,128,512]{2,1,0:T(8,128)(2,1)S(1)} %copy.28), channel_id=1, replica_groups={{0,2,4,6},{8,10,12,14},{16,18,20,22},{24,26,28,30},{1,3,5,7},{9,11,13,1..., dimensions={0} | all-to-all | bytes 1048576 | tf_op jit(solution)/shard_map/all_to_all | solution.py:54
  23.0 8.1 %all_to_all.41 = bf16[4,128,256]{1,2,0:T(8,128)(2,1)S(1)} all-to-all(bf16[4,128,256]{1,2,0:T(8,128)(2,1)S(1)} %bitcast.78), channel_id=1, replica_groups={{0,2,4,6},{8,10,12,14},{16,18,20,22},{24,26,28,30},{1,3,5,7},{9,11,13,1..., dimensions={0} | all-to-all | bytes 524288 | tf_op jit(solution)/shard_map/all_to_all | solution.py:54
  31.1 0.9 copy.29
  32.0 0.7 copy.30
  32.7 14.2 %all_to_all.42 = bf16[4,128,1024]{1,2,0:T(8,128)(2,1)S(1)} all-to-all(bf16[4,128,1024]{1,2,0:T(8,128)(2,1)S(1)} %bitcast.68), channel_id=1, replica_groups={{0,2,4,6},{8,10,12,14},{16,18,20,22},{24,26,28,30},{1,3,5,7},{9,11,13,1..., dimensions={0} | all-to-all | bytes 2097152 | tf_op jit(solution)/shard_map/all_to_all | solution.py:54
  46.9 1.4 copy.31
  48.4 13.1 %all_to_all.43 = bf16[4,128,1024]{1,2,0:T(8,128)(2,1)S(1)} all-to-all(bf16[4,128,1024]{1,2,0:T(8,128)(2,1)S(1)} %bitcast.74), channel_id=1, replica_groups={{0,2,4,6},{8,10,12,14},{16,18,20,22},{24,26,28,30},{1,3,5,7},{9,11,13,1..., dimensions={0} | all-to-all | bytes 2097152 | tf_op jit(solution)/shard_map/all_to_all | solution.py:54
  61.5 1.3 copy.32
  63.2 1.6 broadcast_in_dim.13
  64.8 3.7 %all-to-all-start.1 = ((bf16[4,128,2048]{2,1,0:T(8,128)(2,1)}), bf16[4,128,2048]{2,1,0:T(8,128)(2,1)S(1)}, u32[]{:S(2)}, u32[]{:S(2)}) async-start(bf16[4,128,2048]{2,1,0:T(8,128)(2,1)} %broadcast_in_dim.13), calls=%async_computation.1 | async-start | bytes 4194304 | tf_op jit(solution)/shard_map/all_to_all | solution.py:54
  68.7 1.8 all-gather
  71.2 17.7 %all-to-all-done.1 = bf16[4,128,2048]{2,1,0:T(8,128)(2,1)S(1)} async-done(((bf16[4,128,2048]{2,1,0:T(8,128)(2,1)}), bf16[4,128,2048]{2,1,0:T(8,128)(2,1)S(1)}, u32[]{:S(2)}, u32[]{:S(2)}) %all-to-all-start.1) | async-done | bytes 2097184 | tf_op jit(solution)/shard_map/all_to_all | solution.py:54
  88.8 4.6 %convolution_bitcast_fusion = f32[2,512,512]{2,1,0:T(8,128)S(1)} fusion(bf16[512,2048,1]{1,0,2:T(8,128)(2,1)S(1)} %bitcast.69, bf16[2,2048,512]{2,1,0:T(8,128)(2,1)} %bitcast.84), kind=kOutput, calls=%fused_computation.34 | convolution fusion | flops 2147483648 | bytes 8388608 | tf_op jit(solution)/shard_map/td,sdn->stn/dot_general | solution.py:119
  93.7 4.6 %fusion.73 = (f32[4,128]{1,0:T(4,128)S(1)}, f32[4,128]{1,0:T(4,128)S(1)}, f32[2,4,128,256]{3,2,1,0:T(8,128)S(1)}) fusion(f32[2,256]{1,0:T(2,128)S(1)} %mul.485, f32[2,256]{1,0:T(2,128)S(1)} %mul.482, f32[2,256]{1,0:T(2,128)S(1)} %mul.479, f32[2,256]{1,0:T(2,128)S(1)} %mul.476, f32[2,256]{1,0:T(2,128)S(1)} %mul.473, f32[2,256]{1,0:T(2,128)S(1)} %mul.470, ...), kind=kLoop, calls=%fused_computation.158 | loop fusion | flops 16776192 | bytes 2164736 | tf_op jit(solution)/shard_map/reduce_sum | solution.py:123
  98.3 8.9 %all-reduce.1 = (f32[512]{0:T(512)S(1)}, f32[512]{0:T(512)S(1)}) all-reduce(f32[512]{0:T(512)S(1)} %bitcast.80, f32[512]{0:T(512)S(1)} %bitcast.79), channel_id=1, replica_groups={{0,2,4,6},{1,3,5,7},{8,10,12,14},{9,11,13,15},{16,18,20,22},{17,19,21,2..., use_global_device_ids=true, to_apply=%region_4.5 | all-reduce | flops 1024 | bytes 8192 | tf_op jit(solution)/shard_map/psum | solution.py:122
  107.6 3.1 bitcast_convert_fusion.1
  110.7 24.1 %all_to_all.44 = bf16[4,128,2048]{2,1,0:T(8,128)(2,1)S(1)} all-to-all(bf16[4,128,2048]{2,1,0:T(8,128)(2,1)S(1)} %bitcast.72), channel_id=1, replica_groups={{0,2,4,6},{8,10,12,14},{16,18,20,22},{24,26,28,30},{1,3,5,7},{9,11,13,1..., dimensions={0} | all-to-all | bytes 4194304 | tf_op jit(solution)/shard_map/all_to_all | solution.py:54
  134.8 0.4 reduce_sum.69
  135.3 1.3 multiply_reduce_fusion
  136.6 1.3 multiply_convert_fusion.1
  138.1 23.0 %all_to_all.45 = bf16[4,128,2048]{2,1,0:T(8,128)(2,1)S(1)} all-to-all(bf16[4,128,2048]{2,1,0:T(8,128)(2,1)S(1)} %broadcast_in_dim.15), channel_id=1, replica_groups={{0,2,4,6},{8,10,12,14},{16,18,20,22},{24,26,28,30},{1,3,5,7},{9,11,13,1..., dimensions={0} | all-to-all | bytes 4194304 | tf_op jit(solution)/shard_map/all_to_all | solution.py:54
  161.1 21.1 %all-gather.10.cloned.1.call-done = bf16[4096,1024]{1,0:T(8,128)(2,1)} async-done(((bf16[512,1024]{1,0:T(8,128)(2,1)}), bf16[4096,1024]{1,0:T(8,128)(2,1)}) %all-gather.10.cloned.1.call-update) | async-done | bytes 8388624 | tf_op jit(solution)/shard_map/all_gather | solution.py:60
  182.3 82.0 %all-gather.12.cloned.1.call-done = bf16[4096,1024]{1,0:T(8,128)(2,1)} async-done(((bf16[512,1024]{1,0:T(8,128)(2,1)}), bf16[4096,1024]{1,0:T(8,128)(2,1)}) %all-gather.12.cloned.1.call-update) | async-done | bytes 8388624 | tf_op jit(solution)/shard_map/all_gather | solution.py:60
  264.3 15.9 %bitcast_convert_fusion = bf16[512,2048]{1,0:T(8,128)(2,1)} fusion(bf16[2,2048,1024]{2,1,0:T(8,128)(2,1)} %bitcast.83, bf16[512,2048,1]{1,0,2:T(8,128)(2,1)S(1)} %bitcast.71, bf16[2,2048,1024]{2,1,0:T(8,128)(2,1)} %bitcast.82), kind=kOutput, calls=%fused_computation | convolution fusion | flops 8594128896 | bytes 20971520 | tf_op jit(solution)/shard_map/stf,sdf->td/dot_general | solution.py:145
  280.2 3.6 %all-to-all-start.7 = ((bf16[4,128,2048]{2,1,0:T(8,128)(2,1)}), bf16[4,128,2048]{2,1,0:T(8,128)(2,1)S(1)}, u32[]{:S(2)}, u32[]{:S(2)}) async-start(bf16[4,128,2048]{2,1,0:T(8,128)(2,1)} %bitcast.70), calls=%async_computation.7 | async-start | bytes 4194304 | tf_op jit(solution)/shard_map/all_to_all | solution.py:54
  283.9 25.5 %all-to-all-done.7 = bf16[4,128,2048]{2,1,0:T(8,128)(2,1)S(1)} async-done(((bf16[4,128,2048]{2,1,0:T(8,128)(2,1)}), bf16[4,128,2048]{2,1,0:T(8,128)(2,1)S(1)}, u32[]{:S(2)}, u32[]{:S(2)}) %all-to-all-start.7) | async-done | bytes 2097184 | tf_op jit(solution)/shard_map/all_to_all | solution.py:54
  309.4 0.4 reduce_sum.71
  309.9 1.3 bitcast_dynamic-update-slice_fusion.1
  311.3 1.9 collective-permute-done
  313.3 1.0 copy-done.3
  (75 shorter events, 2.8 us)
Async XLA Ops:
  6.5 82.3 %all-gather.6.cloned.1.call-start = ((), (), s32[]{:S(2)}) async-start(), calls=%async_computation.8 | async-start | bytes 4718592 | tf_op jit(solution)/shard_map/all_gather | solution.py:60
  7.7 15.3 %copy-start.4 = (bf16[1024,128]{1,0:T(8,128)(2,1)S(1)}, bf16[1024,128]{1,0:T(8,128)(2,1)}, u32[]{:S(2)}) copy-start(bf16[1024,128]{1,0:T(8,128)(2,1)} %param.16) | copy-start | bytes 786436
  8.9 23.1 %copy-start.1 = (bf16[128,4096]{1,0:T(8,128)(2,1)S(1)}, bf16[128,4096]{1,0:T(8,128)(2,1)}, u32[]{:S(2)}) copy-start(bf16[128,4096]{1,0:T(8,128)(2,1)} %param.18) | copy-start | bytes 3145732
  22.9 84.7 %all-gather.8.cloned.1.call-start = ((), (), s32[]{:S(2)}) async-start(), calls=%async_computation.9 | async-start | bytes 2359296 | tf_op jit(solution)/shard_map/all_gather | solution.py:60
  31.9 150.3 %all-gather.10.cloned.1.call-start = ((), (), s32[]{:S(2)}) async-start(), calls=%async_computation.10 | async-start | bytes 9437184 | tf_op jit(solution)/shard_map/all_gather | solution.py:60
  46.9 1.5 copy-start.2
  48.3 216.0 %all-gather.12.cloned.1.call-start = ((), (), s32[]{:S(2)}) async-start(), calls=%async_computation.11 | async-start | bytes 9437184 | tf_op jit(solution)/shard_map/all_gather | solution.py:60
  61.5 1.4 copy-start
  61.5 1.6 copy-start.6
  64.8 3.8 %copy-start.5 = (f32[31,1024]{1,0:T(8,128)S(1)}, f32[31,1024]{1,0:T(8,128)}, u32[]{:S(2)}) copy-start(f32[31,1024]{1,0:T(8,128)} %param.14) | copy-start | bytes 380932
  64.8 3.8 %copy-start.8 = (f32[1024]{0:T(1024)S(1)}, f32[1024]{0:T(1024)}, u32[]{:S(2)}) copy-start(f32[1024]{0:T(1024)} %param.15) | copy-start | bytes 12292
  64.8 24.0 %all-to-all-start.1 = ((bf16[4,128,2048]{2,1,0:T(8,128)(2,1)}), bf16[4,128,2048]{2,1,0:T(8,128)(2,1)S(1)}, u32[]{:S(2)}, u32[]{:S(2)}) async-start(bf16[4,128,2048]{2,1,0:T(8,128)(2,1)} %broadcast_in_dim.13), calls=%async_computation.1 | async-start | bytes 4194304 | tf_op jit(solution)/shard_map/all_to_all | solution.py:54
  134.8 1.7 copy-start.7
  280.2 29.1 %all-to-all-start.7 = ((bf16[4,128,2048]{2,1,0:T(8,128)(2,1)}), bf16[4,128,2048]{2,1,0:T(8,128)(2,1)S(1)}, u32[]{:S(2)}, u32[]{:S(2)}) async-start(bf16[4,128,2048]{2,1,0:T(8,128)(2,1)} %bitcast.70), calls=%async_computation.7 | async-start | bytes 4194304 | tf_op jit(solution)/shard_map/all_to_all | solution.py:54
  311.2 2.0 collective-permute-start
  313.3 1.0 copy-start.3
Sparse Core Ops, SparseCore 0:
  23.0 46.5 all-gather.5
  71.2 27.9 all-gather.7
  100.8 81.4 all-gather.9
  183.7 80.5 all-gather.11
